TPU v7x, 32 devices: a whole 2x2x4 slice. The times are simulated.
32 devices in a mesh: sp: 4 (over y, x), tp: 8 (over z, core).
Axes of the slice: x: 2, y: 2, z: 4, core: 2. Of those that a mesh axis runs over, the one named last changes fastest.
Arguments:
- skip_stream_entry: bfloat16 [2048, 2048], P(('sp', 'tp')), may hold values from -6 to 6
- result_switch_mapped: bfloat16 [2048, 4096], P('sp', 'tp'), may hold values from -6 to 6
- channel_feed_mapped: bfloat16 [2048, 4096], P('sp', 'tp'), may hold values from -6 to 6
- write_coefficient_mapped: bfloat16 [2048, 2048], P('sp', 'tp'), may hold values from -6 to 6
- emission_coefficient_mapped: bfloat16 [2048, 2048], P('sp', 'tp'), may hold values from -6 to 6
- channel_feed_taps: bfloat16 [5, 4096], P(None, 'tp'), may hold values from -2.5 to 2.5
- write_coefficient_taps: bfloat16 [5, 2048], P(None, 'tp'), may hold values from -2.5 to 2.5
- emission_coefficient_taps: bfloat16 [5, 2048], P(None, 'tp'), may hold values from -2.5 to 2.5
- raw_increments: bfloat16 [2, 64, 2048], P(None, 'tp', 'sp'), may hold values from -6 to 6
- channel_log_fade_speed: float32 [2, 64], P(None, 'tp'), may hold values from -20 to 0
- extra_log_fade: float32 [2, 64, 2048], P(None, 'tp', 'sp'), may hold values from -1 to 0
- cluster_scaling_factor: float32 [4096], P('tp'), may hold values from 0.1 to 1.9
- blend_result_matrix: bfloat16 [4096, 2048], P('tp'), may hold values from -0.09375 to 0.09375
- routing_scaling_factor: float32 [2048], replicated, may hold values from 0.1 to 1.9
- specialist_switch_matrix: bfloat16 [8, 2048, 4096], P('sp', None, 'tp'), may hold values from -0.125 to 0.125
- specialist_widen_matrix: bfloat16 [8, 2048, 4096], P('sp', None, 'tp'), may hold values from -0.125 to 0.125
- specialist_contract_matrix: bfloat16 [8, 4096, 2048], P('sp', 'tp'), may hold values from -0.1875 to 0.1875
- picked_specialists: int32 [2048, 2], P(('sp', 'tp')), may hold values from 0 to 7, all different within a row; in each aligned block of 64 rows (0 to 63, 64 to 127, ...) at most 24 rows name the same one
- router_affinities: float32 [2048, 2], P(('sp', 'tp')), may hold values from 0.1 to 1
Outputs:
- result: bfloat16 [2048, 2048], P(('sp', 'tp'))
Inputs may be any that keep to these rules, and one draw needn't show every extreme that they name: `picked_specialists`: each row names 2 different experts. Within the rows of one device (aligned blocks of 64 rows) no expert is named more than 24 times, a bound that some block reaches.
All inputs are finite; a program needn't handle non-finite values.
Results may differ from a plain program's by a relative error of at most 0.02.
Values may be sent and summed in bfloat16 or wider, within the bound.
No kernel may reach another device: no remote copies, remote signals or barrier semaphores. Data moves between devices by JAX's collectives and lax.ppermute only.
A program may use at most 64 MiB of HBM per device.

v0:
```python
import jax
import jax.numpy as jnp
from jax import lax
from jax.sharding import PartitionSpec as P

WIDTH = 2048
HEAD_DIM = 64
GROUPS = 16
STATE = 128
CONV_W = 5
BLOCK = 128
TOP = 2
INNER = 4096
EPSILON = 1e-06
HIGHEST_MODE = lax.Precision.HIGHEST


def with_halo(block, sides, width):
    for axis, dim in sides:
        count = lax.axis_size(axis)
        forward = [(i, i + 1) for i in range(count - 1)]
        backward = [(target, source) for source, target in forward]
        low = lax.ppermute(
            lax.slice_in_dim(block, block.shape[dim] - width, None, axis=dim), axis, forward
        )
        high = lax.ppermute(lax.slice_in_dim(block, 0, width, axis=dim), axis, backward)
        block = jnp.concatenate([low, block, high], axis=dim)
    return block


def prefix(shard, axis, combine, identity, reverse):
    peers, here = (lax.axis_size(axis), lax.axis_index(axis))
    everything = jax.tree.map(
        lambda part, kind: lax.all_gather(part.astype(kind), axis),
        shard,
        (jnp.bfloat16, jnp.bfloat16),
    )
    start = jax.tree.map(
        lambda part, zero: jnp.broadcast_to(jnp.asarray(zero, part.dtype), part.shape),
        shard,
        identity,
    )

    def hop(k, before):
        at = peers - 1 - k if reverse else k
        reached = at > here if reverse else at < here
        new = combine(
            before, jax.tree.map(lambda part, own: part[at].astype(own.dtype), everything, shard)
        )
        return jax.tree.map(lambda a, b: jnp.where(reached, a, b), new, before)

    return lax.fori_loop(0, peers, hop, start)


def centred_conv(padded, weights, series_count):
    summed = jnp.zeros((series_count, padded.shape[1]), jnp.float32)
    for offset in range(weights.shape[0]):
        summed = summed + weights[offset].astype(jnp.float32) * padded[
            offset : offset + series_count
        ].astype(jnp.float32)
    return jax.nn.silu(summed)


def local_sweep(inputs, entry_state, readout_state, log_fade_factor, softplus_increment):
    seq_len = inputs.shape[0]
    blocks = seq_len // BLOCK
    heads_here = log_fade_factor.shape[0]
    groups_here = entry_state.shape[1] // STATE
    per_group = heads_here // groups_here
    values = inputs.reshape(blocks, BLOCK, groups_here, per_group, HEAD_DIM)
    b_blocks = entry_state.reshape(blocks, BLOCK, groups_here, STATE)
    c_blocks = readout_state.reshape(blocks, BLOCK, groups_here, STATE)
    decay_blocks = log_fade_factor.reshape(groups_here, per_group, blocks, BLOCK)
    step_blocks = softplus_increment.reshape(groups_here, per_group, blocks, BLOCK)
    cumulative = jnp.cumsum(decay_blocks, axis=-1)
    group_inner = jnp.einsum("bign,bjgn->gbij", c_blocks, b_blocks, precision=HIGHEST_MODE)
    spread = cumulative[..., :, None] - cumulative[..., None, :]
    lower_tri = jnp.arange(BLOCK)[:, None] >= jnp.arange(BLOCK)[None, :]
    mixing = (
        jnp.exp(jnp.where(lower_tri, spread, -jnp.inf))
        * step_blocks[..., None, :]
        * group_inner[:, None]
    )
    within = jnp.einsum("gkbij,bjgkp->bigkp", mixing, values, precision=HIGHEST_MODE)
    to_end = jnp.exp(cumulative[..., -1:] - cumulative) * step_blocks
    block_states = jnp.einsum(
        "gkbj,bjgkp,bjgn->bgkpn", to_end, values, b_blocks, precision=HIGHEST_MODE
    )
    block_decay = cumulative[..., -1]

    def advance(carried, pieces):
        state_piece, decay_piece = pieces
        return (carried * jnp.exp(decay_piece)[..., None, None] + state_piece, carried)

    zero_state = jnp.zeros((groups_here, per_group, HEAD_DIM, STATE), jnp.float32)
    final_state, entering = lax.scan(
        advance, zero_state, (block_states, jnp.moveaxis(block_decay, -1, 0))
    )
    before = jnp.cumsum(block_decay, axis=-1) - block_decay
    return (
        (within, entering, cumulative, before, c_blocks),
        (jnp.sum(block_decay, axis=-1), final_state),
    )


def finish_sweep(parts, carried):
    within, entering, cumulative, before, c_blocks = parts
    entering = entering + carried[None] * jnp.exp(jnp.moveaxis(before, -1, 0))[..., None, None]
    readout = jnp.einsum("bign,bgkpn->bigkp", c_blocks, entering, precision=HIGHEST_MODE)
    readout = readout * jnp.exp(jnp.transpose(cumulative, (2, 3, 0, 1)))[..., None]
    combined = within + readout
    return combined.reshape(combined.shape[0] * combined.shape[1], -1)


def blend_parts_list(
    channel_feed_bordered,
    write_coefficient_bordered,
    emission_coefficient_bordered,
    channel_feed_taps,
    write_coefficient_taps,
    emission_coefficient_taps,
    raw_increments,
    channel_log_fade_speed,
    extra_log_fade,
    series_count,
):
    inputs = centred_conv(channel_feed_bordered, channel_feed_taps, series_count)
    entry_state = centred_conv(write_coefficient_bordered, write_coefficient_taps, series_count)
    readout_state = centred_conv(
        emission_coefficient_bordered, emission_coefficient_taps, series_count
    )
    softplus_increment = jax.nn.softplus(raw_increments.astype(jnp.float32))
    log_fade_factor = (
        -softplus_increment * jnp.exp(channel_log_fade_speed)[..., None] + extra_log_fade
    )
    onward_pass = local_sweep(
        inputs, entry_state, readout_state, log_fade_factor[0], softplus_increment[0]
    )
    backward_pass = local_sweep(
        jnp.flip(inputs, 0),
        jnp.flip(entry_state, 0),
        jnp.flip(readout_state, 0),
        jnp.flip(log_fade_factor[1], -1),
        jnp.flip(softplus_increment[1], -1),
    )
    return (onward_pass, backward_pass)


def gated_norm(mixed_sum, result_switch_mapped, cluster_scaling_factor):
    gated = mixed_sum * jax.nn.silu(result_switch_mapped.astype(jnp.float32))
    grouped = gated.reshape(gated.shape[0], -1, INNER // GROUPS)
    normalized = grouped * lax.rsqrt(jnp.mean(grouped * grouped, axis=-1, keepdims=True) + EPSILON)
    return (normalized.reshape(gated.shape) * cluster_scaling_factor).astype(jnp.bfloat16)


def rms_scale(stream, gain):
    values = stream.astype(jnp.float32)
    return (
        values * lax.rsqrt(jnp.mean(values * values, axis=-1, keepdims=True) + EPSILON) * gain
    ).astype(jnp.bfloat16)


def link_states(former, latter):
    former_total, former_state = former
    latter_total, latter_state = latter
    return (
        former_total + latter_total,
        former_state * jnp.exp(latter_total)[..., None, None] + latter_state,
    )


def per_device(
    skip_stream_entry,
    result_switch_mapped,
    channel_feed_mapped,
    write_coefficient_mapped,
    emission_coefficient_mapped,
    channel_feed_taps,
    write_coefficient_taps,
    emission_coefficient_taps,
    raw_increments,
    channel_log_fade_speed,
    extra_log_fade,
    cluster_scaling_factor,
    blend_result_matrix,
    routing_scaling_factor,
    specialist_switch_matrix,
    specialist_widen_matrix,
    specialist_contract_matrix,
    picked_specialists,
    router_affinities,
):
    series_count = channel_feed_mapped.shape[0]
    rim_width = CONV_W // 2
    sources = (channel_feed_mapped, write_coefficient_mapped, emission_coefficient_mapped)
    edges = jnp.concatenate(
        [jnp.concatenate([source[:rim_width], source[-rim_width:]], 0) for source in sources], 1
    )
    rimmed = with_halo(edges, (("sp", 0),), rim_width)
    padded_list = []
    column_start = 0
    for source in sources:
        width_here = source.shape[1]
        upper_rim = rimmed[:rim_width, column_start : column_start + width_here]
        lower_rim = rimmed[-rim_width:, column_start : column_start + width_here]
        padded_list.append(jnp.concatenate([upper_rim, source, lower_rim], 0))
        column_start = column_start + width_here
    onward_pass, backward_pass = blend_parts_list(
        padded_list[0],
        padded_list[1],
        padded_list[2],
        channel_feed_taps,
        write_coefficient_taps,
        emission_coefficient_taps,
        raw_increments,
        channel_log_fade_speed,
        extra_log_fade,
        series_count,
    )
    fwd_total, fwd_final = onward_pass[1]
    bwd_total, bwd_final = backward_pass[1]
    identity_pair = (jnp.zeros_like(fwd_total), jnp.zeros_like(fwd_final))
    carried_fwd = prefix((fwd_total, fwd_final), "sp", link_states, identity_pair, False)[1]
    carried_bwd = prefix((bwd_total, bwd_final), "sp", link_states, identity_pair, True)[1]
    mixed_sum = finish_sweep(onward_pass[0], carried_fwd) + jnp.flip(
        finish_sweep(backward_pass[0], carried_bwd), 0
    )
    mixed_rows = gated_norm(mixed_sum, result_switch_mapped, cluster_scaling_factor)
    rows_here = skip_stream_entry.shape[0]
    projected = lax.psum_scatter(
        jnp.dot(mixed_rows, blend_result_matrix, preferred_element_type=jnp.float32).astype(
            jnp.bfloat16
        ),
        "tp",
        scatter_dimension=0,
        tiled=True,
    ).astype(jnp.float32)
    after_mixer = (skip_stream_entry.astype(jnp.float32) + projected).astype(jnp.bfloat16)
    normed = rms_scale(after_mixer, routing_scaling_factor)
    experts_here = specialist_switch_matrix.shape[0]
    expert_count = experts_here * lax.axis_size("sp")
    capacity = max(2, 3 * TOP * rows_here // (2 * expert_count))
    slot_total = capacity * expert_count
    flat_routes = picked_specialists.reshape(-1)
    one_hot = (flat_routes[:, None] == jnp.arange(expert_count, dtype=jnp.int32)[None, :]).astype(
        jnp.int32
    )
    earlier_count = jnp.cumsum(one_hot, axis=0) - one_hot
    slot_rank = jnp.sum(earlier_count * one_hot, axis=1)
    position = slot_rank * expert_count + flat_routes
    slot_match = (position[:, None] == jnp.arange(slot_total, dtype=jnp.int32)[None, :]).astype(
        jnp.bfloat16
    )
    buffer = jnp.einsum(
        "rks,rd->sd",
        slot_match.reshape(rows_here, TOP, slot_total),
        normed,
        preferred_element_type=jnp.float32,
    ).astype(jnp.bfloat16)
    buffer = buffer.reshape(capacity, expert_count, WIDTH)
    received = lax.all_to_all(buffer, "sp", split_axis=1, concat_axis=0, tiled=True)
    data_block = lax.all_gather(received, "tp", axis=0, tiled=True)
    gate_part = jnp.einsum(
        "red,edf->ref", data_block, specialist_switch_matrix, preferred_element_type=jnp.float32
    )
    up_part = jnp.einsum(
        "red,edf->ref", data_block, specialist_widen_matrix, preferred_element_type=jnp.float32
    )
    hidden = (jax.nn.silu(gate_part) * up_part).astype(jnp.bfloat16)
    expert_out = lax.psum_scatter(
        jnp.einsum(
            "ref,efd->red", hidden, specialist_contract_matrix, preferred_element_type=jnp.float32
        ).astype(jnp.bfloat16),
        "tp",
        scatter_dimension=0,
        tiled=True,
    )
    returned = lax.all_to_all(expert_out, "sp", split_axis=0, concat_axis=1, tiled=True)
    picked = jnp.dot(
        slot_match, returned.reshape(slot_total, WIDTH), preferred_element_type=jnp.float32
    )
    weights = router_affinities / jnp.sum(router_affinities, axis=-1, keepdims=True)
    mixture = jnp.sum(weights[..., None] * picked.reshape(rows_here, TOP, WIDTH), axis=1)
    return (after_mixer.astype(jnp.float32) + mixture).astype(jnp.bfloat16)


def solution(mesh):
    in_specs = (
        P(("sp", "tp"), None),
        P("sp", "tp"),
        P("sp", "tp"),
        P("sp", "tp"),
        P("sp", "tp"),
        P(None, "tp"),
        P(None, "tp"),
        P(None, "tp"),
        P(None, "tp", "sp"),
        P(None, "tp"),
        P(None, "tp", "sp"),
        P("tp"),
        P("tp", None),
        P(),
        P("sp", None, "tp"),
        P("sp", None, "tp"),
        P("sp", "tp", None),
        P(("sp", "tp"), None),
        P(("sp", "tp"), None),
    )
    out_specs = P(("sp", "tp"), None)
    return jax.shard_map(
        per_device, mesh=mesh, in_specs=in_specs, out_specs=out_specs, check_vma=False
    )
```

profile of v0, /device:TPU:0, one launch (start us, length us, event | category | flops | bytes accessed | tf_op | source)
XLA Modules:
  0.0 437.1 jit_solution(5094532863845228223)
XLA Ops:
  9.1 5.6 %collective-permute-start = (bf16[2,1024]{0,1:T(8,128)(2,1)}, bf16[2,1024]{0,1:T(8,128)(2,1)}, u32[]{:S(2)}, u32[]{:S(2)}) collective-permute-start(bf16[2,1024]{0,1:T(8,128)(2,1)} %copy.175), channel_id=1, source_target_pairs={{0,8},{8,16},{16,24},{1,9},{9,17},{17,25},{2,10},{10,18},{18,26},{... | collective-permute-start | bytes 12296 | tf_op jit(solution)/shard_map/ppermute | solution.py:23
  30.8 9.6 %all-gather.4 = bf16[4,2,4]{2,1,0:T(2,128)(2,1)} all-gather(bf16[1,2,4]{2,1,0:T(2,128)(2,1)S(1)} %bitcast.210), channel_id=2, replica_groups=mesh['sp'=4,'tp'=8] {'sp'}, dimensions={0}, use_global_device_ids=true | all-gather | bytes 80 | tf_op jit(solution)/shard_map/all_gather | solution.py:34
  40.5 8.3 %all-gather.5 = bf16[4,2,4]{2,1,0:T(2,128)(2,1)} all-gather(bf16[1,2,4]{2,1,0:T(2,128)(2,1)S(1)} %bitcast.211), channel_id=4, replica_groups=mesh['sp'=4,'tp'=8] {'sp'}, dimensions={0}, use_global_device_ids=true | all-gather | bytes 80 | tf_op jit(solution)/shard_map/all_gather | solution.py:34
  66.7 4.7 %rev.24 = f32[512,256]{1,0:T(8,128)} reverse(f32[512,256]{1,0:T(8,128)} %divide_multiply_fusion.2), dimensions={0} | reverse | bytes 1048576 | tf_op jit(solution)/shard_map/jit(_flip)/rev | solution.py:142
  76.8 4.7 %rev.25 = f32[512,256]{1,0:T(8,128)} reverse(f32[512,256]{1,0:T(8,128)} %divide_multiply_fusion.1), dimensions={0} | reverse | bytes 1048576 | tf_op jit(solution)/shard_map/jit(_flip)/rev | solution.py:141
  83.4 4.7 %divide_multiply_fusion = f32[512,512]{0,1:T(8,128)} fusion(bf16[512,512]{0,1:T(8,128)(2,1)} %copy.176, bf16[2,512]{0,1:T(8,128)(2,1)S(1)} %slice.207, bf16[2,512]{0,1:T(8,128)(2,1)S(1)} %slice.203, f32[512]{0:T(512)S(1)} %bitcast.198, f32[512]{0:T(512)S(1)} %bitcast.199, f32[512]{0:T(512)S(1)} %bitcast.196, f32[512]{0:T(512)S(1)} %bitcast.197, ...), kind=kLoop, calls=%fused_computation.78 | loop fusion | flops 7864320 | bytes 1587200 | tf_op jit(solution)/shard_map/jit(silu)/mul | solution.py:61
  90.7 9.4 %rev.21 = f32[512,512]{0,1:T(8,128)} reverse(f32[512,512]{0,1:T(8,128)} %divide_multiply_fusion), dimensions={0} | reverse | bytes 2097152 | tf_op jit(solution)/shard_map/jit(_flip)/rev | solution.py:140
  108.0 9.8 %while.56 = (s32[]{:T(128)}, f32[2,4,64,128]{3,2,1,0:T(8,128)S(1)}, f32[4,2,4,64,128]{4,3,2,1,0:T(8,128)}, f32[4,2,4]{2,1,0:T(2,128)}, f32[4,2,4,64,128]{4,3,2,1,0:T(8,128)}, /*index=5*/s32[]{:T(128)}, s32[]{:T(128)}) while((s32[]{:T(128)}, f32[2,4,64,128]{3,2,1,0:T(8,128)S(1)}, f32[4,2,4,64,128]{4,3,2,1,0:T(8,128)}, ...), condition=%wide.region_2.3_spmd.clone, body=%wide.region_1.2_spmd.clone.sunk | while | flops 262147 | bytes 1311424 | solution.py:96
  117.8 10.1 %all-gather.1 = bf16[8,4,64,128]{3,2,1,0:T(8,128)(2,1)} all-gather(bf16[2,4,64,128]{3,2,1,0:T(8,128)(2,1)S(1)} %convert_element_type.229), channel_id=3, replica_groups=mesh['sp'=4,'tp'=8] {'sp'}, dimensions={0}, use_global_device_ids=true | all-gather | bytes 655360 | tf_op jit(solution)/shard_map/all_gather | solution.py:34
  127.9 6.8 %while.57 = (s32[]{:T(128)}, f32[2,4,64,128]{3,2,1,0:T(8,128)S(1)}, s32[]{:T(128)}, bf16[4,2,4]{2,1,0:T(2,128)(2,1)}, bf16[4,2,4,64,128]{4,3,2,1,0:T(8,128)(2,1)}, /*index=5*/s32[]{:T(128)}, s32[]{:T(128)}) while((s32[]{:T(128)}, f32[2,4,64,128]{3,2,1,0:T(8,128)S(1)}, s32[]{:T(128)}, bf16[4,2,4]{2,1,0:T(2,128)(2,1)}, ...), condition=%wide.region_5.6_spmd.clone, body=%wide.region_4.5_spmd.clone.sunk | while | flops 327692 | bytes 655545 | solution.py:52
  134.8 5.6 %fusion.20 = f32[4,128,2,4,64]{1,4,3,2,0:T(8,128)S(1)} fusion(f32[4,128,2,4,64]{1,0,4,3,2:T(4,128)} %reshape.174, f32[2,4,128,128]{3,2,0,1:T(8,128)} %fusion.72, f32[2,4,4,128]{3,1,0,2:T(4,128)S(1)} %bitcast.194, f32[2,4,4,128]{3,1,0,2:T(4,128)S(1)} %copy-done.21, pred[128,128]{1,0:T(8,128)(4,1)S(1)} %copy-done.19), kind=kOutput, calls=%fused_computation.37 | convolution fusion | flops 404750336 | bytes 2670592 | tf_op jit(solution)/shard_map/gkbij,bjgkp->bigkp/dot_general | solution.py:84
  157.1 9.8 %while.58 = (s32[]{:T(128)}, f32[2,4,64,128]{3,2,1,0:T(8,128)S(1)}, f32[4,2,4,64,128]{4,3,2,1,0:T(8,128)}, f32[4,2,4]{2,1,0:T(2,128)}, f32[4,2,4,64,128]{4,3,2,1,0:T(8,128)}, /*index=5*/s32[]{:T(128)}, s32[]{:T(128)}) while((s32[]{:T(128)}, f32[2,4,64,128]{3,2,1,0:T(8,128)S(1)}, f32[4,2,4,64,128]{4,3,2,1,0:T(8,128)}, ...), condition=%wide.region_9.10_spmd.clone, body=%wide.region_8.9_spmd.clone.sunk | while | flops 262147 | bytes 1311424 | solution.py:96
  166.9 10.7 %all-gather.3 = bf16[8,4,64,128]{3,2,1,0:T(8,128)(2,1)} all-gather(bf16[2,4,64,128]{3,2,1,0:T(8,128)(2,1)S(1)} %convert_element_type.232), channel_id=5, replica_groups=mesh['sp'=4,'tp'=8] {'sp'}, dimensions={0}, use_global_device_ids=true | all-gather | bytes 655360 | tf_op jit(solution)/shard_map/all_gather | solution.py:34
  177.6 6.8 %while.59 = (s32[]{:T(128)}, f32[2,4,64,128]{3,2,1,0:T(8,128)S(1)}, s32[]{:T(128)}, bf16[4,2,4]{2,1,0:T(2,128)(2,1)}, bf16[4,2,4,64,128]{4,3,2,1,0:T(8,128)(2,1)...) while((s32[]{:T(128)}, f32[2,4,64,128]{3,2,1,0:T(8,128)S(1)}, s32[]{:T(128)}, ...), condition=%wide.region_12.13_spmd.clone, body=%wide.region_11.12_spmd.clone.sunk | while | flops 327696 | bytes 655607 | solution.py:52
  184.4 5.6 %fusion.23 = f32[4,128,2,4,64]{1,4,3,2,0:T(8,128)S(1)} fusion(f32[4,128,2,4,64]{1,0,4,3,2:T(4,128)} %reshape.178, f32[2,4,128,128]{3,2,0,1:T(8,128)} %fusion.69, f32[2,4,4,128]{3,1,0,2:T(4,128)S(1)} %bitcast.193, f32[2,4,4,128]{3,1,0,2:T(4,128)S(1)} %copy-done.20, pred[128,128]{1,0:T(8,128)(4,1)S(1)} %copy-done.19), kind=kOutput, calls=%fused_computation.38 | convolution fusion | flops 404750336 | bytes 2670592 | tf_op jit(solution)/shard_map/gkbij,bjgkp->bigkp/dot_general | solution.py:84
  192.1 6.0 %rev.26 = f32[512,512]{0,1:T(8,128)} reverse(f32[512,512]{0,1:T(8,128)S(1)} %bitcast.183), dimensions={0} | reverse | bytes 2097152 | tf_op jit(solution)/shard_map/jit(_flip)/rev | solution.py:225
  204.2 35.4 %reduce-scatter.3.cloned.1.call-done = bf16[64,2048]{1,0:T(8,128)(2,1)} async-done(((bf16[512,2048]{1,0:T(8,128)(2,1)}), bf16[64,2048]{1,0:T(8,128)(2,1)}) %reduce-scatter.3.cloned.1.call-update) | async-done | bytes 262160 | tf_op jit(solution)/shard_map/reduce_scatter | solution.py:230
  242.6 12.0 %all_to_all.33 = bf16[24,8,2048]{2,0,1:T(8,128)(2,1)S(1)} all-to-all(bf16[24,8,2048]{2,0,1:T(8,128)(2,1)S(1)} %copy.213), channel_id=1, replica_groups=mesh['sp'=4,'tp'=8] {'sp'}, dimensions={1} | all-to-all | bytes 1572864 | tf_op jit(solution)/shard_map/all_to_all | solution.py:261
  255.9 63.8 %all-gather.8.cloned.1.call-done = bf16[768,2,2048]{2,0,1:T(8,128)(2,1)} async-done(((bf16[96,2,2048]{2,0,1:T(8,128)(2,1)}), bf16[768,2,2048]{2,0,1:T(8,128)(2,1)}) %all-gather.8.cloned.1.call-update) | async-done | bytes 6291472 | tf_op jit(solution)/shard_map/all_gather | solution.py:262
  319.7 9.1 %fusion.107 = f32[2,768,512]{2,1,0:T(8,128)} fusion(bf16[768,2,2048]{2,0,1:T(8,128)(2,1)} %all-gather.8.cloned.1.call-done, bf16[2,2048,512]{2,1,0:T(8,128)(2,1)} %param.42), kind=kOutput, calls=%fused_computation.197 | convolution fusion | flops 3221225472 | bytes 13631488 | tf_op jit(solution)/shard_map/red,edf->ref/dot_general | solution.py:266
  328.7 12.5 %convert_bitcast_fusion = bf16[768,2,2048]{2,0,1:T(8,128)(2,1)} fusion(bf16[2,512,2048]{2,1,0:T(8,128)(2,1)} %param.43, f32[2,768,512]{2,1,0:T(8,128)} %fusion.107, bf16[768,2,2048]{2,0,1:T(8,128)(2,1)} %all-gather.8.cloned.1.call-done, bf16[2,2048,512]{2,1,0:T(8,128)(2,1)} %param.41), kind=kOutput, calls=%fused_computation.12 | convolution fusion | flops 6450315264 | bytes 24117248 | tf_op jit(solution)/shard_map/ref,efd->red/dot_general | solution.py:271
  341.2 68.5 %reduce-scatter.5.cloned.1.call-done = bf16[96,2,2048]{2,0,1:T(8,128)(2,1)} async-done(((bf16[768,2,2048]{2,0,1:T(8,128)(2,1)}), bf16[96,2,2048]{2,0,1:T(8,128)(2,1)}) %reduce-scatter.5.cloned.1.call-update) | async-done | bytes 786448 | tf_op jit(solution)/shard_map/reduce_scatter | solution.py:270
  412.6 3.8 all-to-all-start.1
  416.4 9.1 %all-to-all-done.1 = bf16[96,2,2048]{2,1,0:T(2,128)(2,1)S(1)} async-done(((bf16[96,2,2048]{2,1,0:T(2,128)(2,1)}), bf16[96,2,2048]{2,1,0:T(2,128)(2,1)S(1)}, u32[]{:S(2)}, u32[]{:S(2)}) %all-to-all-start.1) | async-done | bytes 786464 | tf_op jit(solution)/shard_map/all_to_all | solution.py:278
  (211 shorter events, 124.0 us)
Async XLA Ops:
  6.5 193.9 %copy-start = (bf16[512,2048]{1,0:T(8,128)(2,1)S(1)}, bf16[512,2048]{1,0:T(8,128)(2,1)}, u32[]{:S(2)}) copy-start(bf16[512,2048]{1,0:T(8,128)(2,1)} %param.39) | copy-start | bytes 6291460
  6.5 56.1 %copy-start.9 = (bf16[512,256]{1,0:T(8,128)(2,1)S(1)}, bf16[512,256]{1,0:T(8,128)(2,1)}, u32[]{:S(2)}) copy-start(bf16[512,256]{1,0:T(8,128)(2,1)} %param.31) | copy-start | bytes 786436
  6.5 233.0 %reduce-scatter.3.cloned.1.call-start = ((), (), s32[]{:S(2)}) async-start(), calls=%async_computation.4 | async-start | bytes 2359296 | tf_op jit(solution)/shard_map/reduce_scatter | solution.py:230
  9.1 49.0 %collective-permute-start = (bf16[2,1024]{0,1:T(8,128)(2,1)}, bf16[2,1024]{0,1:T(8,128)(2,1)}, u32[]{:S(2)}, u32[]{:S(2)}) collective-permute-start(bf16[2,1024]{0,1:T(8,128)(2,1)} %copy.175), channel_id=1, source_target_pairs={{0,8},{8,16},{16,24},{1,9},{9,17},{17,25},{2,10},{10,18},{18,26},{... | collective-permute-start | bytes 12296 | tf_op jit(solution)/shard_map/ppermute | solution.py:23
  15.5 44.0 %collective-permute-start.1 = (bf16[2,1024]{0,1:T(8,128)(2,1)}, bf16[2,1024]{0,1:T(8,128)(2,1)}, u32[]{:S(2)}, u32[]{:S(2)}) collective-permute-start(bf16[2,1024]{0,1:T(8,128)(2,1)} %copy.178), channel_id=1, source_target_pairs={{8,0},{16,8},{24,16},{9,1},{17,9},{25,17},{10,2},{18,10},{26,18},{... | collective-permute-start | bytes 12296 | tf_op jit(solution)/shard_map/ppermute | solution.py:26
  64.5 18.8 %copy-start.23 = (f32[1,512]{1,0:T(1,128)S(1)}, f32[1,512]{1,0:T(1,128)}, u32[]{:S(2)}) copy-start(f32[1,512]{1,0:T(1,128)} %get-tuple-element.481) | copy-start | bytes 6148
  64.5 18.9 %copy-start.24 = (f32[1,512]{1,0:T(1,128)S(1)}, f32[1,512]{1,0:T(1,128)}, u32[]{:S(2)}) copy-start(f32[1,512]{1,0:T(1,128)} %get-tuple-element.482) | copy-start | bytes 6148
  64.6 18.9 %copy-start.25 = (f32[1,512]{1,0:T(1,128)S(1)}, f32[1,512]{1,0:T(1,128)}, u32[]{:S(2)}) copy-start(f32[1,512]{1,0:T(1,128)} %get-tuple-element.483) | copy-start | bytes 6148
  64.6 18.9 %copy-start.26 = (f32[1,512]{1,0:T(1,128)S(1)}, f32[1,512]{1,0:T(1,128)}, u32[]{:S(2)}) copy-start(f32[1,512]{1,0:T(1,128)} %get-tuple-element.484) | copy-start | bytes 6148
  64.6 18.9 %copy-start.27 = (f32[1,512]{1,0:T(1,128)S(1)}, f32[1,512]{1,0:T(1,128)}, u32[]{:S(2)}) copy-start(f32[1,512]{1,0:T(1,128)} %get-tuple-element.485) | copy-start | bytes 6148
  88.1 15.3 %copy-start.10 = (f32[4,128,2,4]{1,0,3,2:T(4,128)S(1)}, f32[4,128,2,4]{1,0,3,2:T(4,128)}, u32[]{:S(2)}) copy-start(f32[4,128,2,4]{1,0,3,2:T(4,128)} %get-tuple-element.476) | copy-start | bytes 49156
  117.8 17.0 %copy-start.16 = (f32[1,8,512]{2,1,0:T(8,128)S(1)}, f32[1,8,512]{2,1,0:T(8,128)}, u32[]{:S(2)}) copy-start(f32[1,8,512]{2,1,0:T(8,128)} %copy-done.15) | copy-start | bytes 49156
  117.8 17.0 %copy-start.19 = (pred[128,128]{1,0:T(8,128)(4,1)S(1)}, pred[128,128]{1,0:T(8,128)(4,1)}, u32[]{:S(2)}) copy-start(pred[128,128]{1,0:T(8,128)(4,1)} %iota_compare_fusion.3) | copy-start | bytes 49156
  117.8 17.0 %copy-start.21 = (f32[2,4,4,128]{3,1,0,2:T(4,128)S(1)}, f32[2,4,4,128]{3,1,0,2:T(4,128)}, u32[]{:S(2)}) copy-start(f32[2,4,4,128]{3,1,0,2:T(4,128)} %copy.180) | copy-start | bytes 49156
  166.9 17.5 %copy-start.14 = (f32[8,512]{1,0:T(8,128)S(1)}, f32[8,512]{1,0:T(8,128)}, u32[]{:S(2)}) copy-start(f32[8,512]{1,0:T(8,128)} %copy-done.13) | copy-start | bytes 49156
  166.9 17.5 %copy-start.20 = (f32[2,4,4,128]{3,1,0,2:T(4,128)S(1)}, f32[2,4,4,128]{3,1,0,2:T(4,128)}, u32[]{:S(2)}) copy-start(f32[2,4,4,128]{3,1,0,2:T(4,128)} %copy.197) | copy-start | bytes 49156
  200.5 39.1 %copy-start.7 = (bf16[64,2048]{1,0:T(8,128)(2,1)S(1)}, bf16[64,2048]{1,0:T(8,128)(2,1)}, u32[]{:S(2)}) copy-start(bf16[64,2048]{1,0:T(8,128)(2,1)} %param.27) | copy-start | bytes 786436
  200.5 40.3 %copy-start.22 = (f32[2048]{0:T(1024)S(1)}, f32[2048]{0:T(1024)}, u32[]{:S(2)}) copy-start(f32[2048]{0:T(1024)} %param.40) | copy-start | bytes 24580
  203.1 116.5 %all-gather.8.cloned.1.call-start = ((), (), s32[]{:S(2)}) async-start(), calls=%async_computation.5 | async-start | bytes 7077888 | tf_op jit(solution)/shard_map/all_gather | solution.py:262
  255.6 154.2 %reduce-scatter.5.cloned.1.call-start = ((), (), s32[]{:S(2)}) async-start(), calls=%async_computation.6 | async-start | bytes 7077888 | tf_op jit(solution)/shard_map/reduce_scatter | solution.py:270
  341.2 75.2 %copy-start.29 = (f32[64,2]{0,1:T(2,128)S(1)}, f32[64,2]{0,1:T(2,128)}, u32[]{:S(2)}) copy-start(f32[64,2]{0,1:T(2,128)} %param.45) | copy-start | bytes 1540
  412.6 17.2 %copy-start.8 = (bf16[64,2048]{1,0:T(8,128)(2,1)S(1)}, bf16[64,2048]{1,0:T(8,128)(2,1)}, u32[]{:S(2)}) copy-start(bf16[64,2048]{1,0:T(8,128)(2,1)} %reduce-scatter.3.cloned.1.call-done) | copy-start | bytes 786436
  412.6 12.9 %all-to-all-start.1 = ((bf16[96,2,2048]{2,1,0:T(2,128)(2,1)}), bf16[96,2,2048]{2,1,0:T(2,128)(2,1)S(1)}, u32[]{:S(2)}, u32[]{:S(2)}) async-start(bf16[96,2,2048]{2,1,0:T(2,128)(2,1)} %copy.215), calls=%async_computation.3 | async-start | bytes 1572864 | tf_op jit(solution)/shard_map/all_to_all | solution.py:278
  416.4 14.2 %copy-start.1 = (bf16[512,2048]{1,0:T(8,128)(2,1)S(1)}, bf16[512,2048]{1,0:T(8,128)(2,1)}, u32[]{:S(2)}) copy-start(bf16[512,2048]{1,0:T(8,128)(2,1)} %param.39) | copy-start | bytes 6291460
  (13 other events, 100.3 us)
Sparse Core Ops, SparseCore 0:
  203.2 36.2 reduce-scatter.2
  255.7 63.9 all-gather.7
  341.3 68.3 reduce-scatter.4
where the time goes:
time: 441 us; the launch traced here: 437 us
  waiting for transfers between devices  177 us (40%)
  local copies, waits for them, and re-layouts  76.9 us (17%)
  other arithmetic  57.6 us (13%)
  blocking collectives  50.7 us (11%)
  matrix products  50.2 us (11%)
  between operations  13.7 us (3%)
  starting transfers between devices  11 us (2%)
    reduce_scatter x1, waiting for transfers between devices, per_device(): lax.psum_scatter(jnp.einsum('ref,efd->red', hidden, specialist_contract_m...  68.5 us
    all_gather x1, waiting for transfers between devices, per_device(): data_block = lax.all_gather(received, 'tp', axis=0, tiled=True)  63.8 us
    all_gather x4, blocking collectives, prefix(): lax.all_gather(part.astype(kind), axis)  38.7 us
    reduce_scatter x1, waiting for transfers between devices, per_device(): lax.psum_scatter(jnp.dot(mixed_rows, blend_result_matrix, preferred_eleme...  35.4 us
    dot_general x1, matrix products, per_device(): jnp.einsum('ref,efd->red', hidden, specialist_contract_matrix, preferred_...  12.5 us
    all_to_all x1, blocking collectives, per_device(): lax.all_to_all(buffer, 'sp', split_axis=1, concat_axis=0, tiled=True)  12 us
    dot_general x2, matrix products, local_sweep(): jnp.einsum('gkbij,bjgkp->bigkp', mixing, values, precision=HIGHEST_MODE)  11.3 us
    mul x3, other arithmetic, centred_conv(): return jax.nn.silu(summed)  9.7 us
  transfers between devices with their start and end apart: 6, of which 4 were waited for; matrix products, arithmetic and copies ran while one was open for 6% of the time, Pallas kernels for 0%

commit v1 on v0

--- a/solution.py
+++ b/solution.py
@@ -259,7 +259,12 @@
     ).astype(jnp.bfloat16)
     buffer = buffer.reshape(capacity, expert_count, WIDTH)
     received = lax.all_to_all(buffer, "sp", split_axis=1, concat_axis=0, tiled=True)
-    data_block = lax.all_gather(received, "tp", axis=0, tiled=True)
+    ring = [received]
+    for hop_ in range(7):
+        ring.append(lax.ppermute(ring[-1], "tp", [(dev, (dev + 1) % 8) for dev in range(8)]))
+    data_block = jnp.roll(
+        jnp.concatenate(ring[::-1], axis=0), (lax.axis_index("tp") + 1) * ring[0].shape[0], axis=0
+    )
     gate_part = jnp.einsum(
         "red,edf->ref", data_block, specialist_switch_matrix, preferred_element_type=jnp.float32
     )

time: 441 us -> 489 us (1.11); the launches traced: 437 us -> 480 us
  waiting for transfers between devices: 177 us -> 204 us
  local copies, waits for them, and re-layouts: 76.9 us -> 91.8 us
    ppermute x0 -> x7, waiting for transfers between devices: none -> 92.8 us  [per_device(): lax.ppermute(ring[-1], 'tp', [(dev, (dev + 1) % 8) for dev in range(8)])]
    all_gather x1 -> x0, waiting for transfers between devices: 63.8 us -> none  [per_device(): data_block = lax.all_gather(received, 'tp', axis=0, tiled=True)]
    unnamed x68 -> x81, local copies, waits for them, and re-layouts: 5.77 us -> 21 us
  transfers between devices with their start and end apart: 6 -> 12, of which waited for: 4 -> 10; matrix products, arithmetic and copies ran while one was open for 6% -> 6% of each run, Pallas kernels for 0% -> 0%
where the time goes in v1:
time: 489 us; the launch traced here: 480 us
  waiting for transfers between devices  204 us (42%)
  local copies, waits for them, and re-layouts  91.8 us (19%)
  other arithmetic  57.5 us (12%)
  blocking collectives  50.7 us (10%)
  matrix products  50.3 us (10%)
  between operations  14.3 us (3%)
  starting transfers between devices  10.8 us (2%)
    ppermute x7, waiting for transfers between devices, per_device(): lax.ppermute(ring[-1], 'tp', [(dev, (dev + 1) % 8) for dev in range(8)])  92.8 us
    reduce_scatter x1, waiting for transfers between devices, per_device(): lax.psum_scatter(jnp.einsum('ref,efd->red', hidden, specialist_contract_m...  66.6 us
    all_gather x4, blocking collectives, prefix(): lax.all_gather(part.astype(kind), axis)  38.8 us
    reduce_scatter x1, waiting for transfers between devices, per_device(): lax.psum_scatter(jnp.dot(mixed_rows, blend_result_matrix, preferred_eleme...  35.4 us
    unnamed x81, local copies, waits for them, and re-layouts  21 us
    dot_general x1, matrix products, per_device(): jnp.einsum('ref,efd->red', hidden, specialist_contract_matrix, preferred_...  12.3 us
    all_to_all x1, blocking collectives, per_device(): lax.all_to_all(buffer, 'sp', split_axis=1, concat_axis=0, tiled=True)  11.9 us
    dot_general x2, matrix products, local_sweep(): jnp.einsum('gkbij,bjgkp->bigkp', mixing, values, precision=HIGHEST_MODE)  11.1 us
  transfers between devices with their start and end apart: 12, of which 10 were waited for; matrix products, arithmetic and copies ran while one was open for 6% of the time, Pallas kernels for 0%

profile of v1, /device:TPU:0, one launch (start us, length us, event | category | flops | bytes accessed | tf_op | source)
XLA Modules:
  0.0 479.5 jit_solution(2227715818287565500)
XLA Ops:
  9.1 5.6 %collective-permute-start = (bf16[2,1024]{0,1:T(8,128)(2,1)}, bf16[2,1024]{0,1:T(8,128)(2,1)}, u32[]{:S(2)}, u32[]{:S(2)}) collective-permute-start(bf16[2,1024]{0,1:T(8,128)(2,1)} %copy.175), channel_id=1, source_target_pairs={{0,8},{8,16},{16,24},{1,9},{9,17},{17,25},{2,10},{10,18},{18,26},{... | collective-permute-start | bytes 12296 | tf_op jit(solution)/shard_map/ppermute | solution.py:23
  30.8 9.9 %all-gather.4 = bf16[4,2,4]{2,1,0:T(2,128)(2,1)} all-gather(bf16[1,2,4]{2,1,0:T(2,128)(2,1)S(1)} %bitcast.210), channel_id=2, replica_groups=mesh['sp'=4,'tp'=8] {'sp'}, dimensions={0}, use_global_device_ids=true | all-gather | bytes 80 | tf_op jit(solution)/shard_map/all_gather | solution.py:34
  40.7 7.4 %all-gather.5 = bf16[4,2,4]{2,1,0:T(2,128)(2,1)} all-gather(bf16[1,2,4]{2,1,0:T(2,128)(2,1)S(1)} %bitcast.211), channel_id=4, replica_groups=mesh['sp'=4,'tp'=8] {'sp'}, dimensions={0}, use_global_device_ids=true | all-gather | bytes 80 | tf_op jit(solution)/shard_map/all_gather | solution.py:34
  90.6 9.4 %rev.21 = f32[512,512]{0,1:T(8,128)} reverse(f32[512,512]{0,1:T(8,128)} %divide_multiply_fusion), dimensions={0} | reverse | bytes 2097152 | tf_op jit(solution)/shard_map/jit(_flip)/rev | solution.py:140
  108.8 9.8 %while.56 = (s32[]{:T(128)}, f32[2,4,64,128]{3,2,1,0:T(8,128)S(1)}, f32[4,2,4,64,128]{4,3,2,1,0:T(8,128)}, f32[4,2,4]{2,1,0:T(2,128)}, f32[4,2,4,64,128]{4,3,2,1,0:T(8,128)}, /*index=5*/s32[]{:T(128)}, s32[]{:T(128)}) while((s32[]{:T(128)}, f32[2,4,64,128]{3,2,1,0:T(8,128)S(1)}, f32[4,2,4,64,128]{4,3,2,1,0:T(8,128)}, ...), condition=%wide.region_2.3_spmd.clone, body=%wide.region_1.2_spmd.clone.sunk | while | flops 262147 | bytes 1311424 | solution.py:96
  118.6 11.2 %all-gather.1 = bf16[8,4,64,128]{3,2,1,0:T(8,128)(2,1)} all-gather(bf16[2,4,64,128]{3,2,1,0:T(8,128)(2,1)S(1)} %convert_element_type.229), channel_id=3, replica_groups=mesh['sp'=4,'tp'=8] {'sp'}, dimensions={0}, use_global_device_ids=true | all-gather | bytes 655360 | tf_op jit(solution)/shard_map/all_gather | solution.py:34
  129.8 6.7 %while.57 = (s32[]{:T(128)}, f32[2,4,64,128]{3,2,1,0:T(8,128)S(1)}, s32[]{:T(128)}, bf16[4,2,4]{2,1,0:T(2,128)(2,1)}, bf16[4,2,4,64,128]{4,3,2,1,0:T(8,128)(2,1)}, /*index=5*/s32[]{:T(128)}, s32[]{:T(128)}) while((s32[]{:T(128)}, f32[2,4,64,128]{3,2,1,0:T(8,128)S(1)}, s32[]{:T(128)}, bf16[4,2,4]{2,1,0:T(2,128)(2,1)}, ...), condition=%wide.region_5.6_spmd.clone, body=%wide.region_4.5_spmd.clone.sunk | while | flops 327692 | bytes 655545 | solution.py:52
  136.6 5.5 %fusion.25 = f32[4,128,2,4,64]{1,4,3,2,0:T(8,128)S(1)} fusion(f32[4,128,2,4,64]{1,0,4,3,2:T(4,128)} %reshape.174, f32[2,4,128,128]{3,2,0,1:T(8,128)} %fusion.79, f32[2,4,4,128]{3,1,0,2:T(4,128)S(1)} %bitcast.194, f32[2,4,4,128]{3,1,0,2:T(4,128)S(1)} %copy-done.24, pred[128,128]{1,0:T(8,128)(4,1)S(1)} %copy-done.22), kind=kOutput, calls=%fused_computation.40 | convolution fusion | flops 404750336 | bytes 2670592 | tf_op jit(solution)/shard_map/gkbij,bjgkp->bigkp/dot_general | solution.py:84
  161.0 9.7 %while.58 = (s32[]{:T(128)}, f32[2,4,64,128]{3,2,1,0:T(8,128)S(1)}, f32[4,2,4,64,128]{4,3,2,1,0:T(8,128)}, f32[4,2,4]{2,1,0:T(2,128)}, f32[4,2,4,64,128]{4,3,2,1,0:T(8,128)}, /*index=5*/s32[]{:T(128)}, s32[]{:T(128)}) while((s32[]{:T(128)}, f32[2,4,64,128]{3,2,1,0:T(8,128)S(1)}, f32[4,2,4,64,128]{4,3,2,1,0:T(8,128)}, ...), condition=%wide.region_9.10_spmd.clone, body=%wide.region_8.9_spmd.clone.sunk | while | flops 262147 | bytes 1311424 | solution.py:96
  170.8 10.3 %all-gather.3 = bf16[8,4,64,128]{3,2,1,0:T(8,128)(2,1)} all-gather(bf16[2,4,64,128]{3,2,1,0:T(8,128)(2,1)S(1)} %convert_element_type.232), channel_id=5, replica_groups=mesh['sp'=4,'tp'=8] {'sp'}, dimensions={0}, use_global_device_ids=true | all-gather | bytes 655360 | tf_op jit(solution)/shard_map/all_gather | solution.py:34
  181.1 6.7 %while.59 = (s32[]{:T(128)}, f32[2,4,64,128]{3,2,1,0:T(8,128)S(1)}, s32[]{:T(128)}, bf16[4,2,4]{2,1,0:T(2,128)(2,1)}, bf16[4,2,4,64,128]{4,3,2,1,0:T(8,128)(2,1)...) while((s32[]{:T(128)}, f32[2,4,64,128]{3,2,1,0:T(8,128)S(1)}, s32[]{:T(128)}, ...), condition=%wide.region_12.13_spmd.clone, body=%wide.region_11.12_spmd.clone.sunk | while | flops 327696 | bytes 655607 | solution.py:52
  196.6 6.0 %rev.26 = f32[512,512]{0,1:T(8,128)} reverse(f32[512,512]{0,1:T(8,128)S(1)} %bitcast.184), dimensions={0} | reverse | bytes 2097152 | tf_op jit(solution)/shard_map/jit(_flip)/rev | solution.py:225
  208.7 35.4 %reduce-scatter.3.cloned.1.call-done = bf16[64,2048]{1,0:T(8,128)(2,1)} async-done(((bf16[512,2048]{1,0:T(8,128)(2,1)}), bf16[64,2048]{1,0:T(8,128)(2,1)}) %reduce-scatter.3.cloned.1.call-update) | async-done | bytes 262160 | tf_op jit(solution)/shard_map/reduce_scatter | solution.py:230
  247.1 11.9 %all_to_all.33 = bf16[24,8,2048]{2,0,1:T(8,128)(2,1)S(1)} all-to-all(bf16[24,8,2048]{2,0,1:T(8,128)(2,1)S(1)} %copy.213), channel_id=1, replica_groups=mesh['sp'=4,'tp'=8] {'sp'}, dimensions={1} | all-to-all | bytes 1572864 | tf_op jit(solution)/shard_map/all_to_all | solution.py:261
  259.1 13.2 %collective-permute-done.2 = bf16[96,2,2048]{2,0,1:T(8,128)(2,1)S(1)} collective-permute-done((bf16[96,2,2048]{2,0,1:T(8,128)(2,1)S(1)}, bf16[96,2,2048]{2,0,1:T(8,128)(2,1)S(1)}, u32[]{:S(2)}, u32[]{:S(2)}) %collective-permute-start.2) | collective-permute-done | bytes 786464 | tf_op jit(solution)/shard_map/ppermute | solution.py:264
  272.3 13.2 %collective-permute-done.3 = bf16[96,2,2048]{2,0,1:T(8,128)(2,1)S(1)} collective-permute-done((bf16[96,2,2048]{2,0,1:T(8,128)(2,1)S(1)}, bf16[96,2,2048]{2,0,1:T(8,128)(2,1)S(1)}, u32[]{:S(2)}, u32[]{:S(2)}) %collective-permute-start.3) | collective-permute-done | bytes 786464 | tf_op jit(solution)/shard_map/ppermute | solution.py:264
  285.5 13.2 %collective-permute-done.4 = bf16[96,2,2048]{2,0,1:T(8,128)(2,1)S(1)} collective-permute-done((bf16[96,2,2048]{2,0,1:T(8,128)(2,1)S(1)}, bf16[96,2,2048]{2,0,1:T(8,128)(2,1)S(1)}, u32[]{:S(2)}, u32[]{:S(2)}) %collective-permute-start.4) | collective-permute-done | bytes 786464 | tf_op jit(solution)/shard_map/ppermute | solution.py:264
  299.6 13.2 %collective-permute-done.5 = bf16[96,2,2048]{2,0,1:T(8,128)(2,1)S(1)} collective-permute-done((bf16[96,2,2048]{2,0,1:T(8,128)(2,1)S(1)}, bf16[96,2,2048]{2,0,1:T(8,128)(2,1)S(1)}, u32[]{:S(2)}, u32[]{:S(2)}) %collective-permute-start.5) | collective-permute-done | bytes 786464 | tf_op jit(solution)/shard_map/ppermute | solution.py:264
  313.7 13.2 %collective-permute-done.6 = bf16[96,2,2048]{2,0,1:T(8,128)(2,1)S(1)} collective-permute-done((bf16[96,2,2048]{2,0,1:T(8,128)(2,1)S(1)}, bf16[96,2,2048]{2,0,1:T(8,128)(2,1)S(1)}, u32[]{:S(2)}, u32[]{:S(2)}) %collective-permute-start.6) | collective-permute-done | bytes 786464 | tf_op jit(solution)/shard_map/ppermute | solution.py:264
  327.9 13.3 %collective-permute-done.7 = bf16[96,2,2048]{2,0,1:T(8,128)(2,1)} collective-permute-done((bf16[96,2,2048]{2,0,1:T(8,128)(2,1)S(1)}, bf16[96,2,2048]{2,0,1:T(8,128)(2,1)}, u32[]{:S(2)}, u32[]{:S(2)}) %collective-permute-start.7) | collective-permute-done | bytes 786464 | tf_op jit(solution)/shard_map/ppermute | solution.py:264
  341.4 13.5 %collective-permute-done.8 = bf16[96,2,2048]{2,0,1:T(8,128)(2,1)} collective-permute-done((bf16[96,2,2048]{2,0,1:T(8,128)(2,1)}, bf16[96,2,2048]{2,0,1:T(8,128)(2,1)}, u32[]{:S(2)}, u32[]{:S(2)}) %collective-permute-start.8) | collective-permute-done | bytes 786464 | tf_op jit(solution)/shard_map/ppermute | solution.py:264
  372.8 12.3 %convert_bitcast_fusion = bf16[768,2,2048]{2,0,1:T(8,128)(2,1)} fusion(bf16[2,512,2048]{2,1,0:T(8,128)(2,1)} %param.43, f32[2,768,512]{2,1,0:T(8,128)} %fusion.4, bf16[2,2048,512]{2,1,0:T(8,128)(2,1)} %param.42, bf16[1536,2,2048]{2,0,1:T(8,128)(2,1)} %copy-done.19, s32[]{:T(128)S(6)} %select_n.81), kind=kOutput, calls=%fused_computation.12 | convolution fusion | flops 6450315264 | bytes 24117252 | tf_op jit(solution)/shard_map/ref,efd->red/dot_general | solution.py:276
  385.2 66.6 %reduce-scatter.5.cloned.1.call-done = bf16[96,2,2048]{2,0,1:T(8,128)(2,1)} async-done(((bf16[768,2,2048]{2,0,1:T(8,128)(2,1)}), bf16[96,2,2048]{2,0,1:T(8,128)(2,1)}) %reduce-scatter.5.cloned.1.call-update) | async-done | bytes 786448 | tf_op jit(solution)/shard_map/reduce_scatter | solution.py:275
  458.3 9.1 %all-to-all-done.1 = bf16[96,2,2048]{2,1,0:T(2,128)(2,1)S(1)} async-done(((bf16[96,2,2048]{2,1,0:T(2,128)(2,1)}), bf16[96,2,2048]{2,1,0:T(2,128)(2,1)S(1)}, u32[]{:S(2)}, u32[]{:S(2)}) %all-to-all-start.1) | async-done | bytes 786464 | tf_op jit(solution)/shard_map/all_to_all | solution.py:283
  (236 shorter events, 171.6 us)
Async XLA Ops:
  6.5 198.4 %copy-start = (bf16[512,2048]{1,0:T(8,128)(2,1)S(1)}, bf16[512,2048]{1,0:T(8,128)(2,1)}, u32[]{:S(2)}) copy-start(bf16[512,2048]{1,0:T(8,128)(2,1)} %param.39) | copy-start | bytes 6291460
  6.5 66.1 %copy-start.11 = (bf16[512,256]{1,0:T(8,128)(2,1)S(1)}, bf16[512,256]{1,0:T(8,128)(2,1)}, u32[]{:S(2)}) copy-start(bf16[512,256]{1,0:T(8,128)(2,1)} %param.30) | copy-start | bytes 786436
  6.5 237.6 %reduce-scatter.3.cloned.1.call-start = ((), (), s32[]{:S(2)}) async-start(), calls=%async_computation.4 | async-start | bytes 2359296 | tf_op jit(solution)/shard_map/reduce_scatter | solution.py:230
  9.1 48.3 %collective-permute-start = (bf16[2,1024]{0,1:T(8,128)(2,1)}, bf16[2,1024]{0,1:T(8,128)(2,1)}, u32[]{:S(2)}, u32[]{:S(2)}) collective-permute-start(bf16[2,1024]{0,1:T(8,128)(2,1)} %copy.175), channel_id=1, source_target_pairs={{0,8},{8,16},{16,24},{1,9},{9,17},{17,25},{2,10},{10,18},{18,26},{... | collective-permute-start | bytes 12296 | tf_op jit(solution)/shard_map/ppermute | solution.py:23
  15.5 43.4 %collective-permute-start.1 = (bf16[2,1024]{0,1:T(8,128)(2,1)}, bf16[2,1024]{0,1:T(8,128)(2,1)}, u32[]{:S(2)}, u32[]{:S(2)}) collective-permute-start(bf16[2,1024]{0,1:T(8,128)(2,1)} %copy.178), channel_id=1, source_target_pairs={{8,0},{16,8},{24,16},{9,1},{17,9},{25,17},{10,2},{18,10},{26,18},{... | collective-permute-start | bytes 12296 | tf_op jit(solution)/shard_map/ppermute | solution.py:26
  72.5 30.6 %copy-start.12 = (f32[4,128,2,4]{1,0,3,2:T(4,128)S(1)}, f32[4,128,2,4]{1,0,3,2:T(4,128)}, u32[]{:S(2)}) copy-start(f32[4,128,2,4]{1,0,3,2:T(4,128)} %get-tuple-element.476) | copy-start | bytes 49156
  108.8 33.4 %copy-start.14 = (f32[4,128,2,4]{1,3,2,0:T(4,128)S(1)}, f32[4,128,2,4]{1,3,2,0:T(4,128)}, u32[]{:S(2)}) copy-start(f32[4,128,2,4]{1,3,2,0:T(4,128)} %copy.195) | copy-start | bytes 49156
  108.8 33.4 %copy-start.21 = (f32[4,2,4]{2,1,0:T(2,128)S(1)}, f32[4,2,4]{2,1,0:T(2,128)}, u32[]{:S(2)}) copy-start(f32[4,2,4]{2,1,0:T(2,128)} %copy.193) | copy-start | bytes 388
  161.0 32.4 %copy-start.13 = (f32[4,128,2,4]{1,3,2,0:T(4,128)S(1)}, f32[4,128,2,4]{1,3,2,0:T(4,128)}, u32[]{:S(2)}) copy-start(f32[4,128,2,4]{1,3,2,0:T(4,128)} %copy.208) | copy-start | bytes 49156
  161.0 32.4 %copy-start.20 = (f32[4,2,4]{2,1,0:T(2,128)S(1)}, f32[4,2,4]{2,1,0:T(2,128)}, u32[]{:S(2)}) copy-start(f32[4,2,4]{2,1,0:T(2,128)} %copy.206) | copy-start | bytes 388
  202.6 41.5 %copy-start.9 = (bf16[64,2048]{1,0:T(8,128)(2,1)S(1)}, bf16[64,2048]{1,0:T(8,128)(2,1)}, u32[]{:S(2)}) copy-start(bf16[64,2048]{1,0:T(8,128)(2,1)} %param.27) | copy-start | bytes 786436
  202.6 42.7 %copy-start.25 = (f32[2048]{0:T(1024)S(1)}, f32[2048]{0:T(1024)}, u32[]{:S(2)}) copy-start(f32[2048]{0:T(1024)} %param.40) | copy-start | bytes 24580
  207.6 244.1 %reduce-scatter.5.cloned.1.call-start = ((), (), s32[]{:S(2)}) async-start(), calls=%async_computation.5 | async-start | bytes 7077888 | tf_op jit(solution)/shard_map/reduce_scatter | solution.py:275
  259.0 13.3 %collective-permute-start.2 = (bf16[96,2,2048]{2,0,1:T(8,128)(2,1)S(1)}, bf16[96,2,2048]{2,0,1:T(8,128)(2,1)S(1)}, u32[]{:S(2)}, u32[]{:S(2)}) collective-permute-start(bf16[96,2,2048]{2,0,1:T(8,128)(2,1)S(1)} %bitcast.176), channel_id=1, source_target_pairs={{0,1},{1,2},{2,3},{3,4},{4,5},{5,6},{6,7},{7,0},{8,9},{9,10},{10,1... | collective-permute-start | bytes 2359304 | tf_op jit(solution)/shard_map/ppermute | solution.py:264
  272.3 13.2 %collective-permute-start.3 = (bf16[96,2,2048]{2,0,1:T(8,128)(2,1)S(1)}, bf16[96,2,2048]{2,0,1:T(8,128)(2,1)S(1)}, u32[]{:S(2)}, u32[]{:S(2)}) collective-permute-start(bf16[96,2,2048]{2,0,1:T(8,128)(2,1)S(1)} %collective-permute-done.2), channel_id=1, source_target_pairs={{0,1},{1,2},{2,3},{3,4},{4,5},{5,6},{6,7},{7,0},{8,9},{9,10},{10,1... | collective-permute-start | bytes 2359304 | tf_op jit(solution)/shard_map/ppermute | solution.py:264
  285.5 13.2 %collective-permute-start.4 = (bf16[96,2,2048]{2,0,1:T(8,128)(2,1)S(1)}, bf16[96,2,2048]{2,0,1:T(8,128)(2,1)S(1)}, u32[]{:S(2)}, u32[]{:S(2)}) collective-permute-start(bf16[96,2,2048]{2,0,1:T(8,128)(2,1)S(1)} %collective-permute-done.3), channel_id=1, source_target_pairs={{0,1},{1,2},{2,3},{3,4},{4,5},{5,6},{6,7},{7,0},{8,9},{9,10},{10,1... | collective-permute-start | bytes 2359304 | tf_op jit(solution)/shard_map/ppermute | solution.py:264
  299.6 13.2 %collective-permute-start.5 = (bf16[96,2,2048]{2,0,1:T(8,128)(2,1)S(1)}, bf16[96,2,2048]{2,0,1:T(8,128)(2,1)S(1)}, u32[]{:S(2)}, u32[]{:S(2)}) collective-permute-start(bf16[96,2,2048]{2,0,1:T(8,128)(2,1)S(1)} %collective-permute-done.4), channel_id=1, source_target_pairs={{0,1},{1,2},{2,3},{3,4},{4,5},{5,6},{6,7},{7,0},{8,9},{9,10},{10,1... | collective-permute-start | bytes 2359304 | tf_op jit(solution)/shard_map/ppermute | solution.py:264
  313.7 13.2 %collective-permute-start.6 = (bf16[96,2,2048]{2,0,1:T(8,128)(2,1)S(1)}, bf16[96,2,2048]{2,0,1:T(8,128)(2,1)S(1)}, u32[]{:S(2)}, u32[]{:S(2)}) collective-permute-start(bf16[96,2,2048]{2,0,1:T(8,128)(2,1)S(1)} %collective-permute-done.5), channel_id=1, source_target_pairs={{0,1},{1,2},{2,3},{3,4},{4,5},{5,6},{6,7},{7,0},{8,9},{9,10},{10,1... | collective-permute-start | bytes 2359304 | tf_op jit(solution)/shard_map/ppermute | solution.py:264
  327.9 13.3 %collective-permute-start.7 = (bf16[96,2,2048]{2,0,1:T(8,128)(2,1)S(1)}, bf16[96,2,2048]{2,0,1:T(8,128)(2,1)}, u32[]{:S(2)}, u32[]{:S(2)}) collective-permute-start(bf16[96,2,2048]{2,0,1:T(8,128)(2,1)S(1)} %collective-permute-done.6), channel_id=1, source_target_pairs={{0,1},{1,2},{2,3},{3,4},{4,5},{5,6},{6,7},{7,0},{8,9},{9,10},{10,1... | collective-permute-start | bytes 2359304 | tf_op jit(solution)/shard_map/ppermute | solution.py:264
  341.2 13.7 %collective-permute-start.8 = (bf16[96,2,2048]{2,0,1:T(8,128)(2,1)}, bf16[96,2,2048]{2,0,1:T(8,128)(2,1)}, u32[]{:S(2)}, u32[]{:S(2)}) collective-permute-start(bf16[96,2,2048]{2,0,1:T(8,128)(2,1)} %collective-permute-done.7), channel_id=1, source_target_pairs={{0,1},{1,2},{2,3},{3,4},{4,5},{5,6},{6,7},{7,0},{8,9},{9,10},{10,1... | collective-permute-start | bytes 2359304 | tf_op jit(solution)/shard_map/ppermute | solution.py:264
  385.1 73.1 %copy-start.27 = (f32[64,2]{0,1:T(2,128)S(1)}, f32[64,2]{0,1:T(2,128)}, u32[]{:S(2)}) copy-start(f32[64,2]{0,1:T(2,128)} %param.45) | copy-start | bytes 1540
  385.1 87.4 %copy-start.1 = (bf16[512,2048]{1,0:T(8,128)(2,1)S(1)}, bf16[512,2048]{1,0:T(8,128)(2,1)}, u32[]{:S(2)}) copy-start(bf16[512,2048]{1,0:T(8,128)(2,1)} %param.39) | copy-start | bytes 6291460
  385.1 86.6 %copy-start.10 = (bf16[64,2048]{1,0:T(8,128)(2,1)S(1)}, bf16[64,2048]{1,0:T(8,128)(2,1)}, u32[]{:S(2)}) copy-start(bf16[64,2048]{1,0:T(8,128)(2,1)} %reduce-scatter.3.cloned.1.call-done) | copy-start | bytes 786436
  454.6 12.7 %all-to-all-start.1 = ((bf16[96,2,2048]{2,1,0:T(2,128)(2,1)}), bf16[96,2,2048]{2,1,0:T(2,128)(2,1)S(1)}, u32[]{:S(2)}, u32[]{:S(2)}) async-start(bf16[96,2,2048]{2,1,0:T(2,128)(2,1)} %copy.215), calls=%async_computation.3 | async-start | bytes 1572864 | tf_op jit(solution)/shard_map/all_to_all | solution.py:283
  (18 other events, 232.0 us)
Sparse Core Ops, SparseCore 0:
  207.7 36.3 reduce-scatter.2
  385.3 66.4 reduce-scatter.4
